TPU v7x, 32 devices: a whole 2x2x4 slice. The times are simulated.
32 devices in a mesh: sp: 8 (over z, x), tp: 4 (over y, core).
Axes of the slice: x: 2, y: 2, z: 4, core: 2. Of those that a mesh axis runs over, the one named last changes fastest.
Arguments:
- inputs: bfloat16 [3072, 2048], P('sp', 'tp'), may hold values from -6 to 6
- norm_gain: float32 [2048], replicated, may hold values from 0.1 to 1.9
- query_weight: bfloat16 [2048, 1024], P(None, 'tp')
- key_weight: bfloat16 [2048, 1024], P(None, 'tp'), may hold values from -0.15625 to 0.15625
- value_weight: bfloat16 [2048, 1024], P(None, 'tp'), may hold values from -0.125 to 0.125
- memory_query_weight: bfloat16 [2048, 1024], P(None, 'tp'), may hold values from -0.125 to 0.125
- memory_key_weight: bfloat16 [2048, 1024], P(None, 'tp'), may hold values from -0.125 to 0.125
- memory_value_weight: bfloat16 [2048, 1024], P(None, 'tp'), may hold values from -0.125 to 0.125
- input_gate_weight: bfloat16 [2048, 16], P(None, 'tp')
- forget_gate_weight: bfloat16 [2048, 16], P(None, 'tp'), may hold values from -0.3125 to 0.3125
- forget_bias: float32 [16], P('tp'), may hold values from 3 to 13
- decay_shift: float32 [3072, 16], P('sp', 'tp'), may hold values from -2 to 0, as said below
- lambdas: float32 [16], P('tp'), may hold values from 0.3 to 0.8
- head_gain: float32 [64], replicated, may hold values from 0.1 to 1.9
- out_weight_attention: bfloat16 [1024, 2048], P('tp'), may hold values from -0.125 to 0.125
- out_weight_memory: bfloat16 [1024, 2048], P('tp'), may hold values from -0.125 to 0.125
Outputs:
- combined: bfloat16 [3072, 2048], P('sp', 'tp')
Inputs may be any that keep to these rules, and one draw needn't show every extreme that they name: `decay_shift`: never positive.
All inputs are finite; a program needn't handle non-finite values.
Results may differ from a plain program's by a relative error of at most 0.018.
The roundings to bfloat16 on the way count: a program that leaves them out, or rounds other values in their place, can miss the bound.
Values may be sent and summed in bfloat16 or wider, within the bound.
A program may use at most 192 MiB of HBM per device.

v0:
```python
import jax
import jax.numpy as jnp
from jax import lax
from jax.sharding import PartitionSpec as P

HEAD = 64
DD = 32
BLOCK = 64
EPSILON = 1e-06
ROTARY_BASE = 10000.0
NEGATIVE = -1e30


def carried_in(part, axis, combine, identity):
    place = lax.axis_index(axis)
    gathered = jax.tree.map(lambda a: lax.all_gather(a, axis), part)
    state = jax.tree.map(lambda a, e: jnp.zeros_like(a) + jnp.asarray(e, a.dtype), part, identity)

    def one(hop, state):
        return combine(
            state, jax.tree.map(lambda a: lax.dynamic_index_in_dim(a, hop, 0, False), gathered)
        )

    return lax.fori_loop(0, place, one, state)


def rotate(halves, positions):
    middle = halves.shape[-1] // 2
    inverse = 1.0 / ROTARY_BASE ** (jnp.arange(middle, dtype=jnp.float32) / middle)
    angles = positions.astype(jnp.float32)[:, None] * inverse[None, :]
    cosine = jnp.cos(angles)[:, None, :]
    sine_part = jnp.sin(angles)[:, None, :]
    floats = halves.astype(jnp.float32)
    former = floats[..., :middle]
    latter = floats[..., middle:]
    turned = jnp.concatenate(
        [former * cosine - latter * sine_part, latter * cosine + former * sine_part], axis=-1
    )
    return turned.astype(jnp.bfloat16)


def advance_state(carried, block_entry):
    memory, normal, stable = carried
    block_memory, block_normal, block_max, block_decay = block_entry
    new_stable = jnp.maximum(block_decay + stable, block_max)
    former = jnp.exp(block_decay + stable - new_stable)
    latter = jnp.exp(block_max - new_stable)
    return (
        former[:, None, None] * memory + latter[:, None, None] * block_memory,
        former[:, None] * normal + latter[:, None] * block_normal,
        new_stable,
    )


def memory_blocks(queries, key_heads, values, gate_in, log_forget, entering):
    token_count, head_count, head_width = queries.shape
    block_count = token_count // BLOCK
    highest = lax.Precision.HIGHEST

    def blocked(flat_array):
        return (
            flat_array.astype(jnp.float32)
            .reshape(block_count, BLOCK, head_count, head_width)
            .transpose(2, 0, 1, 3)
        )

    query_blocks = blocked(queries)
    key_blocks = blocked(key_heads) * head_width ** (-0.5)
    value_blocks = blocked(values)
    gate_blocks = gate_in.reshape(block_count, BLOCK, head_count).transpose(2, 0, 1)
    cumulative = jnp.cumsum(
        log_forget.reshape(block_count, BLOCK, head_count).transpose(2, 0, 1), axis=-1
    )
    block_ends = cumulative[..., -1]
    toward_end = block_ends[..., None] - cumulative + gate_blocks
    local_max = jnp.max(toward_end, axis=-1)
    end_weights = jnp.exp(toward_end - local_max[..., None])
    local_memory = jnp.einsum(
        "hcl,hclv,hclk->chvk", end_weights, value_blocks, key_blocks, precision=highest
    )
    local_normal = jnp.einsum("hcl,hclk->chk", end_weights, key_blocks, precision=highest)

    def scan_step(carried, block_entry):
        return (advance_state(carried, block_entry), carried)

    entries = (local_memory, local_normal, local_max.T, block_ends.T)
    unused, (memory_in, normal_in, stable_in) = lax.scan(scan_step, entering, entries)
    lower_mask = jnp.tril(jnp.ones((BLOCK, BLOCK), dtype=bool))
    decays = jnp.where(
        lower_mask,
        cumulative[..., :, None] - cumulative[..., None, :] + gate_blocks[..., None, :],
        NEGATIVE,
    )
    carried_log = cumulative + stable_in.T[..., None]
    row_max = jnp.maximum(carried_log, jnp.max(decays, axis=-1))
    within = jnp.where(lower_mask, jnp.exp(decays - row_max[..., None]), 0.0)
    outside = jnp.exp(carried_log - row_max)
    scores = within * jnp.einsum("hctd,hcsd->hcts", query_blocks, key_blocks, precision=highest)
    numerator = outside[..., None] * jnp.einsum(
        "chvk,hctk->hctv", memory_in, query_blocks, precision=highest
    )
    numerator = numerator + jnp.einsum("hcts,hcsv->hctv", scores, value_blocks, precision=highest)
    denominator = outside * jnp.einsum(
        "chk,hctk->hct", normal_in, query_blocks, precision=highest
    ) + jnp.sum(scores, axis=-1)
    result = numerator / jnp.maximum(jnp.abs(denominator), 1.0)[..., None]
    return (
        result.transpose(1, 2, 0, 3)
        .reshape(token_count, head_count * head_width)
        .astype(jnp.bfloat16)
    )


def combine_states(earlier, later_part):
    memory, normal, stable, decay_sum = earlier
    later_memory, later_normal, later_stable, later_decay = later_part
    new_stable = jnp.maximum(later_decay + stable, later_stable)
    former = jnp.exp(later_decay + stable - new_stable)
    latter = jnp.exp(later_stable - new_stable)
    return (
        former[:, None, None] * memory + latter[:, None, None] * later_memory,
        former[:, None] * normal + latter[:, None] * later_normal,
        new_stable,
        decay_sum + later_decay,
    )


def summarize(key_heads, values, gate_in, log_forget):
    head_width = key_heads.shape[-1]
    highest = lax.Precision.HIGHEST
    key_floats = key_heads.astype(jnp.float32) * head_width ** (-0.5)
    cumulative = jnp.cumsum(log_forget, axis=0)
    span_decay = cumulative[-1]
    toward_end = span_decay[None, :] - cumulative + gate_in
    span_max = jnp.max(toward_end, axis=0)
    end_weights = jnp.exp(toward_end - span_max[None, :])
    memory = jnp.einsum(
        "rh,rhv,rhk->hvk", end_weights, values.astype(jnp.float32), key_floats, precision=highest
    )
    normal = jnp.einsum("rh,rhk->hk", end_weights, key_floats, precision=highest)
    return (memory, normal, span_max, span_decay)


def attend(carried, arriving, query_first, query_second, query_positions):
    key_first = arriving[..., :DD]
    key_second = arriving[..., DD : 2 * DD]
    value_part = arriving[..., 2 * DD :]
    key_positions = jnp.arange(arriving.shape[0], dtype=jnp.int32)
    visible = (key_positions[None, :] <= query_positions[:, None]) & (key_positions[None, :] >= 0)
    score_scale = DD ** (-0.5)
    results = []
    for side_index, (query_side, key_side) in enumerate(
        ((query_first, key_first), (query_second, key_second))
    ):
        row_max, totals, accumulated = carried[3 * side_index : 3 * side_index + 3]
        scores = (
            jnp.einsum("qhd,khd->hqk", query_side, key_side, preferred_element_type=jnp.float32)
            * score_scale
        )
        scores = jnp.where(visible[None], scores, NEGATIVE)
        new_max = jnp.maximum(row_max, jnp.max(scores, axis=2))
        weights = jnp.where(visible[None], jnp.exp(scores - new_max[..., None]), 0.0)
        totals = jnp.sum(weights, axis=2)
        accumulated = jnp.einsum(
            "hqk,khd->hqd",
            weights.astype(jnp.bfloat16),
            value_part,
            preferred_element_type=jnp.float32,
        )
        results.extend([new_max, totals, accumulated])
    return tuple(results)


def per_device(
    inputs,
    norm_gain,
    query_weight,
    key_weight,
    value_weight,
    memory_query_weight,
    memory_key_weight,
    memory_value_weight,
    input_gate_weight,
    forget_gate_weight,
    forget_bias,
    decay_shift,
    lambdas,
    head_gain,
    out_weight_attention,
    out_weight_memory,
):
    row_count = inputs.shape[0]
    weights = (
        query_weight,
        key_weight,
        value_weight,
        memory_query_weight,
        memory_key_weight,
        memory_value_weight,
        input_gate_weight,
        forget_gate_weight,
    )
    floats = lax.all_gather(inputs, "tp", axis=1, tiled=True).astype(jnp.float32)
    scaled = (floats * norm_gain[None, :]).astype(jnp.bfloat16)
    running_sums = tuple(
        (jnp.dot(scaled, weight, preferred_element_type=jnp.float32) for weight in weights)
    )
    running_sums, squares = (running_sums, jnp.sum(floats * floats, axis=1))
    inverse_rms = lax.rsqrt(squares / norm_gain.shape[0] + EPSILON)[:, None]
    projected = [running * inverse_rms for running in running_sums]

    def split_heads(flat_values):
        return flat_values.astype(jnp.bfloat16).reshape(row_count, -1, HEAD)

    queries = split_heads(projected[0])
    key_heads = split_heads(projected[1])
    values = split_heads(projected[2])
    offset = lax.axis_index("sp") * row_count
    positions = offset + jnp.arange(row_count, dtype=jnp.int32)
    query_first = rotate(queries[..., :DD], positions)
    query_second = rotate(queries[..., DD:], positions)
    packed = jnp.concatenate(
        [rotate(key_heads[..., :DD], positions), rotate(key_heads[..., DD:], positions), values],
        axis=-1,
    )
    head_count = queries.shape[1]
    empty_max = jnp.full((head_count, row_count), NEGATIVE, jnp.float32)
    empty_total = jnp.zeros((head_count, row_count), jnp.float32)
    empty_sums = jnp.zeros((head_count, row_count, HEAD), jnp.float32)
    starting = (empty_max, empty_total, empty_sums, empty_max, empty_total, empty_sums)
    gathered = attend(
        starting,
        lax.all_gather(packed, "sp", axis=0, tiled=True),
        query_first,
        query_second,
        positions,
    )
    first_max, first_total, first_sums, second_max, second_total, second_sums = gathered
    stacked = first_sums / first_total[..., None] - lambdas[:, None, None] * (
        second_sums / second_total[..., None]
    )
    stacked = stacked.transpose(1, 0, 2)
    norm_scale = lax.rsqrt(jnp.mean(stacked * stacked, axis=-1, keepdims=True) + EPSILON)
    attended = (stacked * norm_scale * head_gain).astype(jnp.bfloat16).reshape(row_count, -1)
    gate_in = projected[6]
    log_forget = jax.nn.log_sigmoid(projected[7] + forget_bias[None, :]) + decay_shift
    memory_queries = split_heads(projected[3])
    memory_keys = split_heads(projected[4])
    memory_values = split_heads(projected[5])
    summary = summarize(memory_keys, memory_values, gate_in, log_forget)
    memory_heads = gate_in.shape[1]
    identity = (
        jnp.zeros((memory_heads, HEAD, HEAD), jnp.float32),
        jnp.zeros((memory_heads, HEAD), jnp.float32),
        jnp.full((memory_heads,), NEGATIVE, jnp.float32),
        jnp.zeros((memory_heads,), jnp.float32),
    )
    prefix = carried_in(summary, "sp", combine_states, identity)
    start_state = (
        jnp.zeros((memory_heads, HEAD, HEAD), jnp.float32),
        jnp.zeros((memory_heads, HEAD), jnp.float32),
        jnp.zeros((memory_heads,), jnp.float32),
        jnp.zeros((memory_heads,), jnp.float32),
    )
    entering = combine_states(start_state, prefix)[:3]
    memory = memory_blocks(
        memory_queries, memory_keys, memory_values, gate_in, log_forget, entering
    )
    partial_term = jnp.dot(attended, out_weight_attention, preferred_element_type=jnp.float32)
    partial_term = partial_term + jnp.dot(
        memory, out_weight_memory, preferred_element_type=jnp.float32
    )
    return lax.psum_scatter(
        partial_term.astype(jnp.bfloat16), "tp", scatter_dimension=1, tiled=True
    )


def solution(mesh):
    in_specs = (
        P("sp", "tp"),
        P(),
        P(None, "tp"),
        P(None, "tp"),
        P(None, "tp"),
        P(None, "tp"),
        P(None, "tp"),
        P(None, "tp"),
        P(None, "tp"),
        P(None, "tp"),
        P("tp"),
        P("sp", "tp"),
        P("tp"),
        P(),
        P("tp", None),
        P("tp", None),
    )
    out_specs = P("sp", "tp")
    return jax.shard_map(
        per_device, mesh=mesh, in_specs=in_specs, out_specs=out_specs, check_vma=False
    )
```

profile of v0, /device:TPU:0, one launch (start us, length us, event | category | flops | bytes accessed | tf_op | source)
XLA Modules:
  0.0 310.0 jit_solution(3127829194106254127)
XLA Ops:
  7.4 1.2 dynamic-slice
  10.2 21.1 %all-gather.8.cloned.1.call-done = bf16[384,2048]{1,0:T(8,128)(2,1)} async-done(((bf16[384,512]{1,0:T(8,128)(2,1)}), bf16[384,2048]{1,0:T(8,128)(2,1)}) %all-gather.8.cloned.1.call-update) | async-done | bytes 1572880 | tf_op jit(solution)/shard_map/all_gather | solution.py:203
  31.3 1.8 fusion.26
  33.2 1.9 fusion.113
  35.2 1.2 reduce-window.6
  37.0 2.0 fusion.128
  39.5 21.3 %all-reduce = f32[32]{0:T(128)S(1)} all-reduce(f32[32]{0:T(128)S(1)} %dynamic-update-slice), channel_id=2, replica_groups=mesh['sp'=8,'tp'=4] {'sp'}, use_global_device_ids=true, to_apply=%add | all-reduce | flops 32 | bytes 256
  60.9 16.7 %all-gather.3 = f32[8,1,4]{2,1,0:T(1,128)} all-gather(f32[1,1,4]{2,1,0:T(1,128)S(1)} %bitcast.225), channel_id=1, replica_groups=mesh['sp'=8,'tp'=4] {'sp'}, dimensions={0}, use_global_device_ids=true | all-gather | bytes 144 | tf_op jit(solution)/shard_map/all_gather | solution.py:16
  77.6 0.9 reduce_window_sum.28
  79.6 2.5 fusion.46
  82.5 0.8 copy.55
  83.3 2.5 fusion.49
  85.8 0.9 copy.57
  86.7 1.2 fusion.84
  88.5 26.1 %all-gather.4 = f32[8,4,64]{2,1,0:T(4,128)S(1)} all-gather(f32[1,4,64]{2,1,0:T(4,128)S(1)} %bitcast.221), channel_id=4, replica_groups=mesh['sp'=8,'tp'=4] {'sp'}, dimensions={0}, use_global_device_ids=true | all-gather | bytes 9216 | tf_op jit(solution)/shard_map/all_gather | solution.py:16
  114.6 2.5 fusion.44
  117.2 0.8 fusion.45
  118.1 0.7 copy-done.8
  118.9 1.3 mul.423
  120.2 0.8 fusion.81
  121.0 1.4 convert_multiply_fusion.2
  122.4 2.3 fusion.78
  124.7 36.9 %all-gather.1 = f32[32,64,64]{2,1,0:T(8,128)} all-gather(f32[4,64,64]{2,1,0:T(8,128)S(1)} %copy-done.7), channel_id=3, replica_groups=mesh['sp'=8,'tp'=4] {'sp'}, dimensions={0}, use_global_device_ids=true | all-gather | bytes 589824 | tf_op jit(solution)/shard_map/all_gather | solution.py:16
  162.0 18.5 %while.37 = (s32[]{:T(128)}, f32[4,64,64]{2,1,0:T(8,128)S(1)}, f32[4,64]{1,0:T(4,128)S(1)}, f32[4]{0:T(128)S(1)}, f32[6,4,64,64]{3,2,0,1:T(8,128)}, /*index=5*/f...) while((s32[]{:T(128)}, f32[4,64,64]{2,1,0:T(8,128)S(1)}, ...), condition=%wide.region_14.15_spmd, body=%wide.region_13.14_spmd.sunk | while | flops 49938 | bytes 399745 | solution.py:87
  162.0 0.7 subtract_exponential_fusion.13
  164.1 1.0 fusion.159
  167.2 1.0 fusion.159
  170.3 1.0 fusion.159
  171.3 0.7 subtract_exponential_fusion.13
  173.3 1.0 fusion.159
  176.4 1.0 fusion.159
  179.5 1.0 fusion.159
  180.5 3.1 %fusion.50 = bf16[384,256]{0,1:T(8,128)(2,1)} fusion(bf16[2048,256]{1,0:T(8,128)(2,1)} %param.25, bf16[384,2048]{1,0:T(8,128)(2,1)} %all-gather.8.cloned.1.call-done, f32[2048]{0:T(1024)S(1)} %copy-done.22, f32[384]{0:T(512)S(1)} %copy-done.11), kind=kOutput, calls=%fused_computation.71 | convolution fusion | flops 405209088 | bytes 2827776 | tf_op jit(solution)/shard_map/dot_general | solution.py:206
  183.6 1.8 copy.64
  185.4 1.9 reshape.199
  187.3 1.9 copy.80
  190.1 1.4 fusion.109
  191.5 1.7 fusion.132
  193.3 0.8 convolution_bitcast_fusion
  194.2 0.9 fusion.32
  195.7 2.5 fusion.43
  198.3 10.2 %fusion.75 = f32[4,384,3072]{2,1,0:T(8,128)} fusion(bf16[3072,4,128]{0,2,1:T(8,128)(2,1)} %all-gather.10.cloned.1.call-done, bf16[384,4,16]{0,2,1:T(8,128)(2,1)S(1)} %get-tuple-element.253, bf16[384,4,16]{0,2,1:T(8,128)(2,1)S(1)} %get-tuple-element.254), kind=kOutput, calls=%fused_computation.82 | convolution fusion | flops 302186496 | bytes 19759104 | tf_op jit(solution)/shard_map/qhd,khd->hqk/dot_general | solution.py:157
  208.5 17.6 %fusion.14 = (f32[4,384]{1,0:T(4,128)S(1)}, f32[4,384]{1,0:T(4,128)S(1)}, f32[4,384,3072]{2,1,0:T(8,128)}) fusion(pred[384,3072]{1,0:T(8,128)(4,1)S(1)} %iota_compare_fusion, f32[4,384,3072]{2,1,0:T(8,128)} %fusion.75, bf16[3072,4,128]{0,2,1:T(8,128)(2,1)} %all-gather.10.cloned.1.call-done, bf16[384,4,16]{0,2,1:T(8,128)(2,1)S(1)} %get-tuple-element.246, ...), kind=kOutput, calls=%fused_computation.32 | convolution fusion | flops 330494976 | bytes 39825408 | tf_op jit(solution)/shard_map/qhd,khd->hqk/dot_general | solution.py:157
  226.1 17.6 %fusion.17 = (f32[4,384]{1,0:T(4,128)S(1)}, f32[4,384]{1,0:T(4,128)S(1)}) fusion(f32[4,384,3072]{2,1,0:T(8,128)} %get-tuple-element.257, f32[4,384]{1,0:T(4,128)S(1)} %get-tuple-element.264, pred[384,3072]{1,0:T(8,128)(4,1)} %copy-done.2, f32[4,384]{1,0:T(4,128)S(1)} %get-tuple-element.265, f32[4,384,3072]{2,1,0:T(8,128)} %fusion.75), kind=kLoop, calls=%fused_computation.35 | loop fusion | flops 47182848 | bytes 38952960 | tf_op jit(solution)/shard_map/reduce_sum | solution.py:163
  244.0 8.0 %fusion.68 = f32[384,4,64]{0,2,1:T(8,128)S(1)} fusion(bf16[3072,4,128]{0,2,1:T(8,128)(2,1)} %all-gather.10.cloned.1.call-done, f32[4,384,3072]{2,1,0:T(8,128)S(1)} %copy-done.1, f32[4,384]{1,0:T(4,128)S(1)} %get-tuple-element.265, pred[384,3072]{1,0:T(8,128)(4,1)} %copy-done.2, f32[384,4]{0,1:T(4,128)S(1)} %bitcast.224), kind=kOutput, calls=%fused_computation.79 | convolution fusion | flops 627671040 | bytes 22032384 | tf_op jit(solution)/shard_map/hqk,khd->hqd/dot_general | solution.py:164
  252.0 9.9 %multiply_reduce_fusion = (f32[384,4]{0,1:T(4,128)S(1)}, f32[384,4,64]{0,2,1:T(8,128)S(1)}) fusion(f32[384,4,64]{0,2,1:T(8,128)S(1)} %fusion.68, f32[384,4]{0,1:T(4,128)S(1)} %bitcast.223, bf16[3072,4,128]{0,2,1:T(8,128)(2,1)} %all-gather.10.cloned.1.call-done, f32[4,384,3072]{2,1,0:T(8,128)} %get-tuple-element.257, f32[4,384]{1,0:T(4,128)S(1)} %get-tuple-element.264, ...), kind=kOutput, calls=%fused_computation.97 | convolution fusion | flops 628062720 | bytes 22431760 | tf_op jit(solution)/shard_map/hqk,khd->hqd/dot_general | solution.py:164
  263.1 1.8 add_convert_fusion
  264.9 38.5 %reduce-scatter.2.cloned.1.call-done = bf16[384,512]{1,0:T(8,128)(2,1)} async-done(((bf16[384,2048]{1,0:T(8,128)(2,1)}), bf16[384,512]{1,0:T(8,128)(2,1)}) %reduce-scatter.2.cloned.1.call-update) | async-done | bytes 393232 | tf_op jit(solution)/shard_map/reduce_scatter | solution.py:273
  (152 shorter events, 19.5 us)
Async XLA Ops:
  6.5 255.5 %copy-start = (bf16[256,2048]{1,0:T(8,128)(2,1)S(1)}, bf16[256,2048]{1,0:T(8,128)(2,1)}, u32[]{:S(2)}) copy-start(bf16[256,2048]{1,0:T(8,128)(2,1)} %param.34) | copy-start | bytes 3145732
  6.5 26.6 %copy-start.19 = (f32[2048]{0:T(1024)S(1)}, f32[2048]{0:T(1024)}, u32[]{:S(2)}) copy-start(f32[2048]{0:T(1024)} %param.21) | copy-start | bytes 24580
  6.5 26.6 %copy-start.24 = (f32[384,4]{0,1:T(4,128)S(1)}, f32[384,4]{0,1:T(4,128)}, u32[]{:S(2)}) copy-start(f32[384,4]{0,1:T(4,128)} %param.31) | copy-start | bytes 18436
  6.5 26.6 %copy-start.25 = (f32[4]{0:T(128)S(1)}, f32[4]{0:T(128)}, u32[]{:S(2)}) copy-start(f32[4]{0:T(128)} %param.30) | copy-start | bytes 52
  6.5 26.6 %copy-start.16 = (bf16[2048,4]{0,1:T(4,128)(2,1)S(1)}, bf16[2048,4]{0,1:T(4,128)(2,1)}, u32[]{:S(2)}) copy-start(bf16[2048,4]{0,1:T(4,128)(2,1)} %param.29) | copy-start | bytes 49156
  6.5 30.5 %copy-start.17 = (bf16[2048,4]{0,1:T(4,128)(2,1)S(1)}, bf16[2048,4]{0,1:T(4,128)(2,1)}, u32[]{:S(2)}) copy-start(bf16[2048,4]{0,1:T(4,128)(2,1)} %param.28) | copy-start | bytes 49156
  6.6 24.8 %all-gather.8.cloned.1.call-start = ((), (), s32[]{:S(2)}) async-start(), calls=%async_computation.1 | async-start | bytes 1966080 | tf_op jit(solution)/shard_map/all_gather | solution.py:203
  7.3 191.0 %all-gather.10.cloned.1.call-start = ((), (), s32[]{:S(2)}) async-start(), calls=%async_computation.2 | async-start | bytes 3538944 | tf_op jit(solution)/shard_map/all_gather | solution.py:233
  10.2 198.3 %copy-start.2 = (pred[384,3072]{1,0:T(8,128)(4,1)}, pred[384,3072]{1,0:T(8,128)(4,1)S(1)}, u32[]{:S(2)}) copy-start(pred[384,3072]{1,0:T(8,128)(4,1)S(1)} %iota_compare_fusion) | copy-start | bytes 3538948
  33.2 84.0 %copy-start.10 = (f32[384]{0:T(512)}, f32[384]{0:T(512)S(1)}, u32[]{:S(2)}) copy-start(f32[384]{0:T(512)S(1)} %add_rsqrt_fusion.1) | copy-start | bytes 4612
  82.5 38.5 %copy-start.3 = (bf16[6,64,4,64]{3,2,1,0:T(4,128)(2,1)}, bf16[6,64,4,64]{3,2,1,0:T(4,128)(2,1)S(1)}, u32[]{:S(2)}) copy-start(bf16[6,64,4,64]{3,2,1,0:T(4,128)(2,1)S(1)} %reshape.198) | copy-start | bytes 589828
  82.5 32.1 %copy-start.20 = (f32[2048]{0:T(1024)S(1)}, f32[2048]{0:T(1024)}, u32[]{:S(2)}) copy-start(f32[2048]{0:T(1024)} %param.21) | copy-start | bytes 24580
  86.7 30.5 %copy-start.5 = (bf16[384,2048]{1,0:T(8,128)(2,1)S(1)}, bf16[384,2048]{1,0:T(8,128)(2,1)}, u32[]{:S(2)}) copy-start(bf16[384,2048]{1,0:T(8,128)(2,1)} %all-gather.8.cloned.1.call-done) | copy-start | bytes 4718596
  86.7 30.5 %copy-start.14 = (bf16[2048,256]{1,0:T(8,128)(2,1)S(1)}, bf16[2048,256]{1,0:T(8,128)(2,1)}, u32[]{:S(2)}) copy-start(bf16[2048,256]{1,0:T(8,128)(2,1)} %param.24) | copy-start | bytes 3145732
  86.7 30.5 %copy-start.21 = (f32[2048]{0:T(1024)S(1)}, f32[2048]{0:T(1024)}, u32[]{:S(2)}) copy-start(f32[2048]{0:T(1024)} %param.21) | copy-start | bytes 24580
  118.0 0.7 copy-start.8
  118.8 184.6 %reduce-scatter.2.cloned.1.call-start = ((), (), s32[]{:S(2)}) async-start(), calls=%async_computation.3 | async-start | bytes 1966080 | tf_op jit(solution)/shard_map/reduce_scatter | solution.py:273
  120.2 4.5 %copy-start.7 = (f32[4,64,64]{2,1,0:T(8,128)S(1)}, f32[4,64,64]{2,1,0:T(8,128)}, u32[]{:S(2)}) copy-start(f32[4,64,64]{2,1,0:T(8,128)} %fusion.84) | copy-start | bytes 196612
  161.6 18.9 %copy-start.11 = (f32[384]{0:T(512)S(1)}, f32[384]{0:T(512)}, u32[]{:S(2)}) copy-start(f32[384]{0:T(512)} %copy-done.10) | copy-start | bytes 4612
  161.6 18.9 %copy-start.22 = (f32[2048]{0:T(1024)S(1)}, f32[2048]{0:T(1024)}, u32[]{:S(2)}) copy-start(f32[2048]{0:T(1024)} %param.21) | copy-start | bytes 24580
  180.5 9.6 %copy-start.18 = (f32[6,4,64]{2,1,0:T(4,128)S(1)}, f32[6,4,64]{2,1,0:T(4,128)}, u32[]{:S(2)}) copy-start(f32[6,4,64]{2,1,0:T(4,128)} %get-tuple-element.126) | copy-start | bytes 18436
  183.6 9.7 %copy-start.4 = (bf16[6,64,4,64]{3,2,1,0:T(4,128)(2,1)S(1)}, bf16[6,64,4,64]{3,2,1,0:T(4,128)(2,1)}, u32[]{:S(2)}) copy-start(bf16[6,64,4,64]{3,2,1,0:T(4,128)(2,1)} %copy-done.3) | copy-start | bytes 589828
  189.5 4.7 %copy-start.9 = (bf16[4,6,64,64]{2,3,1,0:T(8,128)(2,1)S(1)}, bf16[4,6,64,64]{2,3,1,0:T(8,128)(2,1)}, u32[]{:S(2)}) copy-start(bf16[4,6,64,64]{2,3,1,0:T(8,128)(2,1)} %copy.80) | copy-start | bytes 589828
  189.5 4.7 %copy-start.15 = (f32[6,4,64,64]{3,2,0,1:T(8,128)S(1)}, f32[6,4,64,64]{3,2,0,1:T(8,128)}, u32[]{:S(2)}) copy-start(f32[6,4,64,64]{3,2,0,1:T(8,128)} %get-tuple-element.125) | copy-start | bytes 1179652
  193.3 2.3 copy-start.12
  193.3 2.3 copy-start.23
  226.1 17.9 %copy-start.1 = (f32[4,384,3072]{2,1,0:T(8,128)S(1)}, f32[4,384,3072]{2,1,0:T(8,128)}, u32[]{:S(2)}) copy-start(f32[4,384,3072]{2,1,0:T(8,128)} %fusion.75) | copy-start | bytes 56623108
  244.0 8.0 %copy-start.26 = (f32[4]{0:T(128)S(1)}, f32[4]{0:T(128)}, u32[]{:S(2)}) copy-start(f32[4]{0:T(128)} %param.32) | copy-start | bytes 52
  252.0 9.9 %copy-start.13 = (f32[64]{0:T(128)S(1)}, f32[64]{0:T(128)}, u32[]{:S(2)}) copy-start(f32[64]{0:T(128)} %param.33) | copy-start | bytes 772
  261.9 1.2 copy-start.6
Sparse Core Ops, SparseCore 0:
  8.9 22.3 all-gather.7
  118.9 66.6 all-gather.9
  265.0 38.3 reduce-scatter.1
where the time goes:
time: 311 us; the launch traced here: 310 us
  blocking collectives  101 us (32%)
  matrix products  75.5 us (24%)
  waiting for transfers between devices  60.4 us (19%)
  other arithmetic  36.2 us (12%)
  local copies, waits for them, and re-layouts  22.1 us (7%)
  between operations  14.4 us (5%)
    all_gather x3, blocking collectives, carried_in(): gathered = jax.tree.map(lambda a: lax.all_gather(a, axis), part)  79.7 us
    reduce_scatter x1, waiting for transfers between devices, per_device(): lax.psum_scatter(partial_term.astype(jnp.bfloat16), 'tp', scatter_dimensi...  38.5 us
    dot_general x2, matrix products, attend(): jnp.einsum('qhd,khd->hqk', query_side, key_side, preferred_element_type=j...  27.8 us
    unnamed x1, blocking collectives  21.3 us
    all_gather x1, waiting for transfers between devices, per_device(): lax.all_gather(inputs, 'tp', axis=1, tiled=True).astype(jnp.float32)  21.1 us
    dot_general x2, matrix products, attend(): jnp.einsum('hqk,khd->hqd', weights.astype(jnp.bfloat16), value_part, pref...  17.9 us
    dot_general x8, matrix products, per_device(): jnp.dot(scaled, weight, preferred_element_type=jnp.float32)  17.7 us
    reduce_sum x1, other arithmetic, attend(): totals = jnp.sum(weights, axis=2)  17.6 us
  transfers between devices with their start and end apart: 3, of which 2 were waited for; matrix products, arithmetic and copies ran while one was open for 14% of the time, Pallas kernels for 0%

commit v1 on v0

--- a/solution.py
+++ b/solution.py
@@ -9,6 +9,28 @@
 EPSILON = 1e-06
 ROTARY_BASE = 10000.0
 NEGATIVE = -1e30
+
+
+def laid_out(tiles, dim):
+    tiles = jnp.moveaxis(tiles, 0, dim)
+    shape = tiles.shape
+    return tiles.reshape(*shape[:dim], shape[dim] * shape[dim + 1], *shape[dim + 2 :])
+
+
+def ring_gather(value, axis, dim):
+    size = lax.axis_size(axis)
+    pairs = [(i, (i + 1) % size) for i in range(size)]
+    back = [(b, a) for a, b in pairs]
+    lower, upper = ([], [])
+    for step in range(size - 1):
+        if step % 2 == 0:
+            lower.append(lax.ppermute(lower[-1] if lower else value, axis, pairs))
+        else:
+            upper.append(lax.ppermute(upper[-1] if upper else value, axis, back))
+    blocks = jnp.stack([*lower[::-1], value, *upper])
+    shift = lax.axis_index(axis) - len(lower)
+    blocks = blocks[(jnp.arange(size) - shift) % size]
+    return laid_out(blocks, dim)
 
 
 def carried_in(part, axis, combine, identity):
@@ -200,7 +222,7 @@
         input_gate_weight,
         forget_gate_weight,
     )
-    floats = lax.all_gather(inputs, "tp", axis=1, tiled=True).astype(jnp.float32)
+    floats = ring_gather(inputs, "tp", 1).astype(jnp.float32)
     scaled = (floats * norm_gain[None, :]).astype(jnp.bfloat16)
     running_sums = tuple(
         (jnp.dot(scaled, weight, preferred_element_type=jnp.float32) for weight in weights)

time: 311 us -> 369 us (1.19)
  other arithmetic: 36.2 us -> 62.3 us
  local copies, waits for them, and re-layouts: 22.1 us -> 44 us
  starting transfers between devices: 0.12 us -> 5.28 us
  matrix products: 75.5 us -> 70.9 us
  blocking collectives: 101 us -> 105 us
  waiting for transfers between devices: 60.4 us -> 64.1 us
    all_gather x1 -> x0, waiting for transfers between devices: 21.1 us -> none  [per_device(): lax.all_gather(inputs, 'tp', axis=1, tiled=True).astype(jnp.float32)]
    reduce_scatter x1, waiting for transfers between devices: 38.5 us -> 56.7 us  [per_device(): lax.psum_scatter(partial_term.astype(jnp.bfloat16), 'tp', scatter_dimensi...]
    dynamic_update_slice x18, local copies, waits for them, and re-layouts: 7.69 us -> 19.4 us  [memory_blocks(): lax.scan(scan_step, entering, entries)]
    add x6, other arithmetic: 0.47 us -> 8.01 us  [advance_state(): former[:, None] * normal + latter[:, None] * block_normal]
    ppermute x0 -> x3, waiting for transfers between devices: none -> 7.37 us  [the longest x2 7.36 us: ring_gather(): lower.append(lax.ppermute(lower[-1] if lower else value, axis, pairs))]
    dot_general x8, matrix products: 17.7 us -> 12.3 us  [per_device(): jnp.dot(scaled, weight, preferred_element_type=jnp.float32)]
    ppermute x0 -> x3, starting transfers between devices: none -> 5.06 us  [the longest x2 3.12 us: ring_gather(): lower.append(lax.ppermute(lower[-1] if lower else value, axis, pairs))]
    convert_element_type x0 -> x2, other arithmetic: none -> 4.35 us  [the longest x1 2.26 us: per_device(): scaled = (floats * norm_gain[None, :]).astype(jnp.bfloat16)]
  transfers between devices with their start and end apart: 3 -> 5, of which waited for: 2 -> 3; matrix products, arithmetic and copies ran while one was open for 14% -> 21% of each run, Pallas kernels for 0% -> 0%
where the time goes in v1:
time: 369 us; the launch traced here: 366 us
  blocking collectives  105 us (28%)
  matrix products  70.9 us (19%)
  waiting for transfers between devices  64.1 us (17%)
  other arithmetic  62.3 us (17%)
  local copies, waits for them, and re-layouts  44 us (12%)
  between operations  14.7 us (4%)
  starting transfers between devices  5.28 us (1%)
    all_gather x3, blocking collectives, carried_in(): gathered = jax.tree.map(lambda a: lax.all_gather(a, axis), part)  81.4 us
    reduce_scatter x1, waiting for transfers between devices, per_device(): lax.psum_scatter(partial_term.astype(jnp.bfloat16), 'tp', scatter_dimensi...  56.7 us
    dot_general x2, matrix products, attend(): jnp.einsum('qhd,khd->hqk', query_side, key_side, preferred_element_type=j...  27.9 us
    unnamed x1, blocking collectives  23.2 us
    dynamic_update_slice x18, local copies, waits for them, and re-layouts, memory_blocks(): lax.scan(scan_step, entering, entries)  19.4 us
    dot_general x2, matrix products, attend(): jnp.einsum('hqk,khd->hqd', weights.astype(jnp.bfloat16), value_part, pref...  17.9 us
    reduce_sum x1, other arithmetic, attend(): totals = jnp.sum(weights, axis=2)  17.6 us
    dot_general x8, matrix products, per_device(): jnp.dot(scaled, weight, preferred_element_type=jnp.float32)  12.3 us
  transfers between devices with their start and end apart: 5, of which 3 were waited for; matrix products, arithmetic and copies ran while one was open for 21% of the time, Pallas kernels for 0%

profile of v1, /device:TPU:0, one launch (start us, length us, event | category | flops | bytes accessed | tf_op | source)
XLA Modules:
  0.0 366.0 jit_solution(16328556847652764098)
XLA Ops:
  7.0 1.9 collective-permute-start.2
  9.0 1.7 iota_compare_fusion
  10.7 5.5 %collective-permute-done = bf16[384,512]{1,0:T(8,128)(2,1)S(1)} collective-permute-done((bf16[384,512]{1,0:T(8,128)(2,1)}, bf16[384,512]{1,0:T(8,128)(2,1)S(1)}, u32[]{:S(2)}, u32[]{:S(2)}) %collective-permute-start) | collective-permute-done | bytes 393248 | tf_op jit(solution)/shard_map/ppermute | solution.py:27
  16.3 2.6 collective-permute-start.1
  21.6 1.9 collective-permute-done.1
  23.5 2.4 pad_maximum_fusion
  25.8 2.1 gather_fusion
  28.3 2.1 convert_bitcast_fusion
  30.4 3.6 copy.74
  34.0 2.3 fusion.26
  39.4 23.2 %all-reduce = f32[32]{0:T(128)S(1)} all-reduce(f32[32]{0:T(128)S(1)} %dynamic-update-slice), channel_id=2, replica_groups=mesh['sp'=8,'tp'=4] {'sp'}, use_global_device_ids=true, to_apply=%add | all-reduce | flops 32 | bytes 256
  63.3 17.0 %all-gather.3 = f32[8,1,4]{2,1,0:T(1,128)} all-gather(f32[1,1,4]{2,1,0:T(1,128)S(1)} %bitcast.246), channel_id=1, replica_groups=mesh['sp'=8,'tp'=4] {'sp'}, dimensions={0}, use_global_device_ids=true | all-gather | bytes 144 | tf_op jit(solution)/shard_map/all_gather | solution.py:38
  82.9 2.0 fusion.46
  86.8 2.7 fusion.45
  89.6 1.4 fusion.44
  93.9 26.9 %all-gather.4 = f32[8,4,64]{2,1,0:T(4,128)} all-gather(f32[1,4,64]{2,1,0:T(4,128)S(1)} %bitcast.245), channel_id=4, replica_groups=mesh['sp'=8,'tp'=4] {'sp'}, dimensions={0}, use_global_device_ids=true | all-gather | bytes 9216 | tf_op jit(solution)/shard_map/all_gather | solution.py:38
  123.9 1.3 mul.425
  125.2 2.1 fusion.81
  127.3 1.6 convert_multiply_fusion.1
  128.9 2.3 fusion.78
  131.2 37.5 %all-gather.1 = f32[32,64,64]{2,1,0:T(8,128)} all-gather(f32[4,64,64]{2,1,0:T(8,128)S(1)} %fusion.84), channel_id=3, replica_groups=mesh['sp'=8,'tp'=4] {'sp'}, dimensions={0}, use_global_device_ids=true | all-gather | bytes 589824 | tf_op jit(solution)/shard_map/all_gather | solution.py:38
  171.8 1.3 multiply_add_fusion.1
  174.1 44.7 %while.37 = (s32[]{:T(128)}, f32[4,64,64]{2,1,0:T(8,128)S(1)}, f32[4,64]{1,0:T(4,128)}, f32[4]{0:T(128)}, f32[6,4,64,64]{3,2,0,1:T(8,128)}, /*index=5*/f32[6,4,6...) while((s32[]{:T(128)}, f32[4,64,64]{2,1,0:T(8,128)S(1)}, ...), condition=%wide.region_14.15_spmd, body=%wide.region_13.14_spmd.sunk | while | flops 49938 | bytes 400769 | solution.py:109
  174.1 1.3 dynamic_update_slice.19
  178.5 1.3 fusion.160
  181.6 1.3 dynamic_update_slice.19
  186.0 1.3 fusion.160
  189.0 1.3 dynamic_update_slice.19
  193.4 1.3 fusion.160
  196.5 1.3 dynamic_update_slice.19
  200.9 1.3 fusion.160
  203.9 1.3 dynamic_update_slice.19
  208.4 1.3 fusion.160
  215.8 1.3 fusion.160
  218.9 2.7 fusion.50
  221.5 1.7 copy.87
  223.3 1.9 reshape.251
  225.2 2.0 copy.103
  227.9 1.4 fusion.101
  229.4 1.7 fusion.124
  233.6 2.0 fusion.43
  235.7 10.3 %fusion.75 = f32[4,384,3072]{2,1,0:T(8,128)} fusion(bf16[3072,4,128]{0,2,1:T(8,128)(2,1)} %all-gather.7.cloned.1.call-done, bf16[384,4,16]{0,2,1:T(8,128)(2,1)S(1)} %get-tuple-element.274, bf16[384,4,16]{0,2,1:T(8,128)(2,1)S(1)} %get-tuple-element.275), kind=kOutput, calls=%fused_computation.85 | convolution fusion | flops 302186496 | bytes 19759104 | tf_op jit(solution)/shard_map/qhd,khd->hqk/dot_general | solution.py:179
  246.1 17.6 %fusion.14 = (f32[4,384]{1,0:T(4,128)S(1)}, f32[4,384]{1,0:T(4,128)S(1)}, f32[4,384,3072]{2,1,0:T(8,128)}) fusion(pred[384,3072]{1,0:T(8,128)(4,1)S(1)} %copy-done.2, f32[4,384,3072]{2,1,0:T(8,128)} %fusion.75, bf16[3072,4,128]{0,2,1:T(8,128)(2,1)} %all-gather.7.cloned.1.call-done, bf16[384,4,16]{0,2,1:T(8,128)(2,1)S(1)} %get-tuple-element.267, ...), kind=kOutput, calls=%fused_computation.33 | convolution fusion | flops 330494976 | bytes 39825408 | tf_op jit(solution)/shard_map/qhd,khd->hqk/dot_general | solution.py:179
  263.7 17.6 %fusion.17 = (f32[4,384]{1,0:T(4,128)S(1)}, f32[4,384]{1,0:T(4,128)S(1)}) fusion(f32[4,384,3072]{2,1,0:T(8,128)} %get-tuple-element.278, f32[4,384]{1,0:T(4,128)S(1)} %get-tuple-element.285, pred[384,3072]{1,0:T(8,128)(4,1)} %iota_compare_fusion, f32[4,384]{1,0:T(4,128)S(1)} %get-tuple-element.286, f32[4,384,3072]{2,1,0:T(8,128)} %fusion.75), kind=kLoop, calls=%fused_computation.36 | loop fusion | flops 47182848 | bytes 38952960 | tf_op jit(solution)/shard_map/reduce_sum | solution.py:185
  281.5 8.0 %fusion.68 = f32[384,4,64]{0,2,1:T(8,128)S(1)} fusion(bf16[3072,4,128]{0,2,1:T(8,128)(2,1)} %all-gather.7.cloned.1.call-done, f32[4,384,3072]{2,1,0:T(8,128)S(1)} %copy-done.1, f32[4,384]{1,0:T(4,128)S(1)} %get-tuple-element.286, pred[384,3072]{1,0:T(8,128)(4,1)} %iota_compare_fusion, f32[384,4]{0,1:T(4,128)S(1)} %bitcast.249), kind=kOutput, calls=%fused_computation.82 | convolution fusion | flops 627671040 | bytes 22032384 | tf_op jit(solution)/shard_map/hqk,khd->hqd/dot_general | solution.py:186
  289.5 9.9 %multiply_reduce_fusion = (f32[384,4]{0,1:T(4,128)S(1)}, f32[384,4,64]{0,2,1:T(8,128)S(1)}) fusion(f32[384,4,64]{0,2,1:T(8,128)S(1)} %fusion.68, f32[384,4]{0,1:T(4,128)S(1)} %bitcast.248, bf16[3072,4,128]{0,2,1:T(8,128)(2,1)} %all-gather.7.cloned.1.call-done, f32[4,384,3072]{2,1,0:T(8,128)} %get-tuple-element.278, f32[4,384]{1,0:T(4,128)S(1)} %get-tuple-element.285, ...), kind=kOutput, calls=%fused_computation.100 | convolution fusion | flops 628062720 | bytes 22431760 | tf_op jit(solution)/shard_map/hqk,khd->hqd/dot_general | solution.py:186
  300.7 1.8 add_convert_fusion
  302.5 56.7 %reduce-scatter.2.cloned.1.call-done = bf16[384,512]{1,0:T(8,128)(2,1)} async-done(((bf16[384,2048]{1,0:T(8,128)(2,1)}), bf16[384,512]{1,0:T(8,128)(2,1)}) %reduce-scatter.2.cloned.1.call-update) | async-done | bytes 393232 | tf_op jit(solution)/shard_map/reduce_scatter | solution.py:295
  (170 shorter events, 56.0 us)
Async XLA Ops:
  6.5 293.1 %copy-start = (bf16[256,2048]{1,0:T(8,128)(2,1)S(1)}, bf16[256,2048]{1,0:T(8,128)(2,1)}, u32[]{:S(2)}) copy-start(bf16[256,2048]{1,0:T(8,128)(2,1)} %param.34) | copy-start | bytes 3145732
  6.5 229.2 %all-gather.7.cloned.1.call-start = ((), (), s32[]{:S(2)}) async-start(), calls=%async_computation.1 | async-start | bytes 3538944 | tf_op jit(solution)/shard_map/all_gather | solution.py:255
  6.5 9.7 %collective-permute-start = (bf16[384,512]{1,0:T(8,128)(2,1)}, bf16[384,512]{1,0:T(8,128)(2,1)S(1)}, u32[]{:S(2)}, u32[]{:S(2)}) collective-permute-start(bf16[384,512]{1,0:T(8,128)(2,1)} %param.20), channel_id=1, source_target_pairs={{0,1},{1,2},{2,3},{3,0},{4,5},{5,6},{6,7},{7,4},{8,9},{9,10},{10,1... | collective-permute-start | bytes 1179656 | tf_op jit(solution)/shard_map/ppermute | solution.py:27
  7.0 14.6 %collective-permute-start.2 = (bf16[384,512]{1,0:T(8,128)(2,1)}, bf16[384,512]{1,0:T(8,128)(2,1)S(1)}, u32[]{:S(2)}, u32[]{:S(2)}) collective-permute-start(bf16[384,512]{1,0:T(8,128)(2,1)} %param.20), channel_id=1, source_target_pairs={{1,0},{2,1},{3,2},{0,3},{5,4},{6,5},{7,6},{4,7},{9,8},{10,9},{11,1... | collective-permute-start | bytes 1179656 | tf_op jit(solution)/shard_map/ppermute | solution.py:29
  16.3 7.2 %collective-permute-start.1 = (bf16[384,512]{1,0:T(8,128)(2,1)S(1)}, bf16[384,512]{1,0:T(8,128)(2,1)S(1)}, u32[]{:S(2)}, u32[]{:S(2)}) collective-permute-start(bf16[384,512]{1,0:T(8,128)(2,1)S(1)} %collective-permute-done), channel_id=1, source_target_pairs={{0,1},{1,2},{2,3},{3,0},{4,5},{5,6},{6,7},{7,4},{8,9},{9,10},{10,1... | collective-permute-start | bytes 1179656 | tf_op jit(solution)/shard_map/ppermute | solution.py:27
  21.6 100.3 %copy-start.6 = (f32[384,16]{0,1:T(8,128)}, f32[384,16]{0,1:T(8,128)S(1)}, u32[]{:S(2)}) copy-start(f32[384,16]{0,1:T(8,128)S(1)} %get-tuple-element.276) | copy-start | bytes 73732
  21.6 100.3 %copy-start.8 = (f32[384,16]{0,1:T(8,128)}, f32[384,16]{0,1:T(8,128)S(1)}, u32[]{:S(2)}) copy-start(f32[384,16]{0,1:T(8,128)S(1)} %get-tuple-element.277) | copy-start | bytes 73732
  30.4 60.7 %copy-start.17 = (f32[384]{0:T(512)}, f32[384]{0:T(512)S(1)}, u32[]{:S(2)}) copy-start(f32[384]{0:T(512)S(1)} %add_rsqrt_fusion.1) | copy-start | bytes 4612
  30.4 3.6 copy-start.22
  34.0 2.3 copy-start.19
  34.0 2.3 copy-start.23
  34.0 2.3 copy-start.24
  34.0 4.5 %copy-start.20 = (bf16[2048,4]{0,1:T(4,128)(2,1)S(1)}, bf16[2048,4]{0,1:T(4,128)(2,1)}, u32[]{:S(2)}) copy-start(bf16[2048,4]{0,1:T(4,128)(2,1)} %param.28) | copy-start | bytes 49156
  39.0 50.5 %copy-start.12 = (f32[6,64,4]{1,0,2:T(8,128)}, f32[6,64,4]{1,0,2:T(8,128)S(1)}, u32[]{:S(2)}) copy-start(f32[6,64,4]{1,0,2:T(8,128)S(1)} %reshape.249) | copy-start | bytes 18436
  81.6 8.0 %copy-start.15 = (f32[4,6,64]{2,1,0:T(8,128)}, f32[4,6,64]{2,1,0:T(8,128)S(1)}, u32[]{:S(2)}) copy-start(f32[4,6,64]{2,1,0:T(8,128)S(1)} %subtract_exponential_fusion.4) | copy-start | bytes 18436
  86.8 2.7 copy-start.26
  89.6 1.5 copy-start.27
  122.9 0.7 copy-start.10
  123.7 235.6 %reduce-scatter.2.cloned.1.call-start = ((), (), s32[]{:S(2)}) async-start(), calls=%async_computation.2 | async-start | bytes 1966080 | tf_op jit(solution)/shard_map/reduce_scatter | solution.py:295
  170.4 2.7 copy-start.3
  171.1 3.0 copy-start.14
  218.8 8.3 %copy-start.21 = (f32[6,4]{1,0:T(8,128)S(1)}, f32[6,4]{1,0:T(8,128)}, u32[]{:S(2)}) copy-start(f32[6,4]{1,0:T(8,128)} %get-tuple-element.124) | copy-start | bytes 292
  218.8 8.5 %copy-start.13 = (f32[6,64,4]{1,0,2:T(8,128)S(1)}, f32[6,64,4]{1,0,2:T(8,128)}, u32[]{:S(2)}) copy-start(f32[6,64,4]{1,0,2:T(8,128)} %copy-done.12) | copy-start | bytes 18436
  218.8 8.5 %copy-start.16 = (pred[64,64]{0,1:T(8,128)(4,1)S(1)}, pred[64,64]{0,1:T(8,128)(4,1)}, u32[]{:S(2)}) copy-start(pred[64,64]{0,1:T(8,128)(4,1)} %iota_compare_fusion.1) | copy-start | bytes 12292
  218.8 9.1 %copy-start.29 = (f32[6,4,64]{2,1,0:T(4,128)S(1)}, f32[6,4,64]{2,1,0:T(4,128)}, u32[]{:S(2)}) copy-start(f32[6,4,64]{2,1,0:T(4,128)} %get-tuple-element.126) | copy-start | bytes 18436
  227.3 3.9 %copy-start.4 = (bf16[6,64,4,64]{3,2,1,0:T(4,128)(2,1)S(1)}, bf16[6,64,4,64]{3,2,1,0:T(4,128)(2,1)}, u32[]{:S(2)}) copy-start(bf16[6,64,4,64]{3,2,1,0:T(4,128)(2,1)} %reshape.250) | copy-start | bytes 589828
  227.3 4.7 %copy-start.11 = (bf16[4,6,64,64]{2,3,1,0:T(8,128)(2,1)S(1)}, bf16[4,6,64,64]{2,3,1,0:T(8,128)(2,1)}, u32[]{:S(2)}) copy-start(bf16[4,6,64,64]{2,3,1,0:T(8,128)(2,1)} %copy.103) | copy-start | bytes 589828
  227.3 4.7 %copy-start.28 = (f32[6,4,64,64]{3,2,0,1:T(8,128)S(1)}, f32[6,4,64,64]{3,2,0,1:T(8,128)}, u32[]{:S(2)}) copy-start(f32[6,4,64,64]{3,2,0,1:T(8,128)} %get-tuple-element.125) | copy-start | bytes 1179652
  231.2 2.4 copy-start.18
  233.0 2.7 copy-start.7
  233.0 2.7 copy-start.9
  235.7 10.4 %copy-start.2 = (pred[384,3072]{1,0:T(8,128)(4,1)S(1)}, pred[384,3072]{1,0:T(8,128)(4,1)}, u32[]{:S(2)}) copy-start(pred[384,3072]{1,0:T(8,128)(4,1)} %iota_compare_fusion) | copy-start | bytes 3538948
  263.7 17.9 %copy-start.1 = (f32[4,384,3072]{2,1,0:T(8,128)S(1)}, f32[4,384,3072]{2,1,0:T(8,128)}, u32[]{:S(2)}) copy-start(f32[4,384,3072]{2,1,0:T(8,128)} %fusion.75) | copy-start | bytes 56623108
  281.5 8.0 %copy-start.30 = (f32[4]{0:T(128)S(1)}, f32[4]{0:T(128)}, u32[]{:S(2)}) copy-start(f32[4]{0:T(128)} %param.32) | copy-start | bytes 52
  289.5 10.0 %copy-start.25 = (f32[64]{0:T(128)S(1)}, f32[64]{0:T(128)}, u32[]{:S(2)}) copy-start(f32[64]{0:T(128)} %param.33) | copy-start | bytes 772
  299.5 1.2 copy-start.5
Sparse Core Ops, SparseCore 0:
  123.8 68.7 all-gather.6
  302.6 56.5 reduce-scatter.1
